TPU v7x, 512 devices: a whole 4x4x16 slice. The times are simulated.
512 devices in a mesh: sp: 16 (over z), dp: 32 (over y, x, core).
Axes of the slice: x: 4, y: 4, z: 16, core: 2. Of those that a mesh axis runs over, the one named last changes fastest.
Arguments:
- tokens: bfloat16 [32, 2048, 2048], P('dp', 'sp'), may hold values from -6 to 6
- receptance_weight: bfloat16 [2048, 1024], P('dp'), may hold values from -0.125 to 0.125
- key_projection_weight: bfloat16 [2048, 1024], P('dp'), may hold values from -0.125 to 0.125
- value_projection_weight: bfloat16 [2048, 1024], P('dp'), may hold values from -0.125 to 0.125
- decay_down_weight: bfloat16 [2048, 256], P('dp'), may hold values from -0.125 to 0.125
- decay_up_weight: bfloat16 [2, 128, 1024], replicated, may hold values from -0.71875 to 0.71875
- decay_floor_level: float32 [2, 1024], replicated, may hold values from -10 to -2.25
- correction_rate_logit: float32 [2, 1024], P(None, 'sp'), may hold values from -4 to 4
- diagonal_address_factor: float32 [2, 1024], P(None, 'sp'), may hold values from -1 to 1
- head_norm_gain: float32 [1024], P('sp'), may hold values from 0.1 to 1.9
Outputs:
- mixed: bfloat16 [32, 2048, 1024], P('dp', 'sp')
All inputs are finite; a program needn't handle non-finite values.
Results may differ from a plain program's by a relative error of at most 0.0056.
The roundings to bfloat16 on the way count: a program that leaves them out, or rounds other values in their place, can miss the bound.
Values may be sent and summed in bfloat16 or wider, within the bound.
No kernel may reach another device: no remote copies, remote signals or barrier semaphores. Data moves between devices by JAX's collectives and lax.ppermute only.
A program may use at most 128 MiB of HBM per device.

v0:
```python
import math
import jax
import jax.numpy as jnp
from jax import lax
from jax.sharding import PartitionSpec as P

SUBSPACE_SIZE = 64


def in_one_piece(arrays, axis, dim, along):
    both = jnp.concatenate(arrays, axis=along)
    result, at, outs = (lax.all_gather(both, axis, axis=dim, tiled=True), 0, [])
    for a in arrays:
        outs.append(lax.slice_in_dim(result, at, at + a.shape[along], axis=along))
        at += a.shape[along]
    return tuple(outs)


def contract(pattern, former, latter):
    return jnp.einsum(pattern, former, latter, precision=lax.Precision.HIGHEST)


def project_rows(totals, pieces, source):
    results = []
    for running, piece in zip(totals, pieces):
        results.append(jnp.dot(source, piece, preferred_element_type=jnp.float32))
    return tuple(results)


def both_ways(content_matrix_full):
    return jnp.stack([content_matrix_full, jnp.flip(content_matrix_full, 0)], 0)


def advance(state, pair):
    transfer_block, inject_block = pair
    later = contract("...ij,...jk->...ik", state, transfer_block) + inject_block
    return (later, state)


def per_device(
    tokens,
    receptance_weight,
    key_projection_weight,
    value_projection_weight,
    decay_down_weight,
    decay_up_weight,
    decay_floor_level,
    correction_rate_logit,
    diagonal_address_factor,
    head_norm_gain,
):
    depth = tokens.shape[2]
    source = tokens.reshape(-1, depth)
    row_count = source.shape[0]
    channels = receptance_weight.shape[1]
    low_width = decay_down_weight.shape[1]
    empty = jnp.zeros((row_count, channels), jnp.float32)
    initial = (empty, empty, empty, jnp.zeros((row_count, low_width), jnp.float32))
    sums = project_rows(
        initial,
        in_one_piece(
            (receptance_weight, key_projection_weight, value_projection_weight, decay_down_weight),
            "dp",
            0,
            1,
        ),
        source,
    )
    receive = sums[0].astype(jnp.bfloat16)
    key_rows = sums[1].astype(jnp.bfloat16)
    value_rows = sums[2].astype(jnp.bfloat16)
    lowered = jnp.tanh(sums[3]).astype(jnp.bfloat16)
    rank = decay_up_weight.shape[1]
    forward_pre = (
        jnp.dot(lowered[:, :rank], decay_up_weight[0], preferred_element_type=jnp.float32)
        + decay_floor_level[0]
    ).astype(jnp.bfloat16)
    backward_pre = (
        jnp.dot(lowered[:, rank:], decay_up_weight[1], preferred_element_type=jnp.float32)
        + decay_floor_level[1]
    ).astype(jnp.bfloat16)
    moved = (
        lax.all_to_all(receive, "sp", split_axis=1, concat_axis=0, tiled=True),
        lax.all_to_all(key_rows, "sp", split_axis=1, concat_axis=0, tiled=True),
        lax.all_to_all(value_rows, "sp", split_axis=1, concat_axis=0, tiled=True),
        lax.all_to_all(forward_pre, "sp", split_axis=1, concat_axis=0, tiled=True),
        lax.all_to_all(backward_pre, "sp", split_axis=1, concat_axis=0, tiled=True),
    )
    length = moved[0].shape[0]
    local_channels = moved[0].shape[1]
    subspace_dimension = SUBSPACE_SIZE
    subspace_batches = local_channels // subspace_dimension
    span = math.gcd(length, 64)
    blocks = length // span

    def by_head(content_matrix_full):
        return content_matrix_full.astype(jnp.float32).reshape(
            length, subspace_batches, subspace_dimension
        )

    def to_blocks(content_matrix_full):
        return jnp.transpose(
            content_matrix_full.reshape(2, blocks, span, subspace_batches, subspace_dimension),
            (0, 3, 1, 2, 4),
        )

    gate_by_subspace = by_head(moved[0])
    address_by_subspace = by_head(moved[1])
    value_per_head = by_head(moved[2])
    amend_strength = jax.nn.sigmoid(correction_rate_logit).reshape(
        2, 1, subspace_batches, subspace_dimension
    )
    normed = address_by_subspace / jnp.sqrt(
        jnp.sum(address_by_subspace * address_by_subspace, -1, keepdims=True) + 1.0
    )
    decay_log = -math.exp(-0.5) * jax.nn.sigmoid(
        jnp.stack([by_head(moved[3]), jnp.flip(by_head(moved[4]), 0)], 0)
    )
    block_rate = jnp.transpose(amend_strength, (0, 2, 1, 3))[:, :, :, None, :]
    probe_matrix_full = to_blocks(both_ways(gate_by_subspace))
    content_matrix_full = to_blocks(both_ways(value_per_head))
    erasers = -to_blocks(both_ways(normed))
    writers = -erasers * block_rate
    rated_keys = to_blocks(both_ways(address_by_subspace)) * block_rate
    log_decay = to_blocks(decay_log)
    inclusive = jnp.cumsum(log_decay, axis=3)
    previous = inclusive - log_decay
    middle = inclusive[:, :, :, span // 2 : span // 2 + 1]
    final = inclusive[:, :, :, span - 1 : span]
    erase_query = erasers * jnp.exp(previous - middle)
    read_query = probe_matrix_full * jnp.exp(inclusive - middle)
    write_key = writers * jnp.exp(middle - inclusive)
    plain_key = rated_keys * jnp.exp(middle - inclusive)
    strict = jnp.tril(jnp.ones((span, span), jnp.bool_), -1)
    lower = jnp.tril(jnp.ones((span, span), jnp.bool_))
    erase_write = jnp.where(strict, contract("...tn,...jn->...tj", erase_query, write_key), 0.0)
    erase_plain = jnp.where(strict, contract("...tn,...jn->...tj", erase_query, plain_key), 0.0)
    read_write = jnp.where(lower, contract("...tn,...jn->...tj", read_query, write_key), 0.0)
    read_plain = jnp.where(lower, contract("...tn,...jn->...tj", read_query, plain_key), 0.0)
    identity = jnp.eye(span, dtype=jnp.float32)
    inverse = lax.linalg.triangular_solve(
        identity - erase_write,
        jnp.broadcast_to(identity, erase_write.shape),
        left_side=True,
        lower=True,
        unit_diagonal=True,
    )
    to_end = jnp.exp(final - inclusive)
    carried = contract("...jt,...jn->...tn", inverse, writers * to_end)
    start_erase = erasers * jnp.exp(previous)
    transfer = contract("...tm,...tn->...mn", start_erase, carried) + jnp.eye(
        subspace_dimension, dtype=jnp.float32
    ) * jnp.exp(final)
    inject = contract(
        "...tv,...tn->...vn",
        content_matrix_full,
        contract("...jt,...jn->...tn", erase_plain, carried) + rated_keys * to_end,
    )
    start_state = jnp.zeros(
        (2, subspace_batches, subspace_dimension, subspace_dimension), jnp.float32
    )
    _, entering = lax.scan(
        advance, start_state, (jnp.moveaxis(transfer, 2, 0), jnp.moveaxis(inject, 2, 0))
    )
    entering = jnp.moveaxis(entering, 0, 2)
    pulled = contract(
        "...tj,...jv->...tv",
        inverse,
        contract("...tk,...vk->...tv", start_erase, entering)
        + contract("...tj,...jv->...tv", erase_plain, content_matrix_full),
    )
    outputs = (
        contract("...tk,...vk->...tv", probe_matrix_full * jnp.exp(inclusive), entering)
        + contract("...tj,...jv->...tv", read_write, pulled)
        + contract("...tj,...jv->...tv", read_plain, content_matrix_full)
    )
    ordered = jnp.transpose(outputs, (0, 2, 3, 1, 4)).reshape(
        2, length, subspace_batches, subspace_dimension
    )
    ordered = jnp.stack([ordered[0], jnp.flip(ordered[1], 0)], 0)
    centred = ordered - jnp.mean(ordered, -1, keepdims=True)
    variance = jnp.mean(centred * centred, -1, keepdims=True)
    gain = head_norm_gain.reshape(1, 1, subspace_batches, subspace_dimension)
    normalized = centred * lax.rsqrt(variance + 0.00064) * gain
    diagonal_extra = diagonal_address_factor.reshape(2, 1, subspace_batches, subspace_dimension)
    diagonal_contribution = (
        jnp.sum(
            gate_by_subspace * address_by_subspace * amend_strength * diagonal_extra,
            -1,
            keepdims=True,
        )
        * value_per_head
    )
    mixed = (
        jnp.sum(normalized + diagonal_contribution, 0)
        .reshape(length, local_channels)
        .astype(jnp.bfloat16)
    )
    returned = lax.all_to_all(mixed, "sp", split_axis=0, concat_axis=1, tiled=True)
    return returned.reshape(1, row_count, channels)


def solution(mesh):
    in_specs = (
        P("dp", "sp", None),
        P("dp", None),
        P("dp", None),
        P("dp", None),
        P("dp", None),
        P(),
        P(),
        P(None, "sp"),
        P(None, "sp"),
        P("sp"),
    )
    out_specs = P("dp", "sp", None)
    return jax.shard_map(
        per_device, mesh=mesh, in_specs=in_specs, out_specs=out_specs, check_vma=False
    )
```

profile of v0, /device:TPU:2, one launch (start us, length us, event | category | flops | bytes accessed | tf_op | source)
XLA Modules:
  0.0 680.4 jit_solution(5575840417447938390)
XLA Ops:
  9.3 86.2 %all-gather.2.cloned.1.call-done = bf16[2048,3328]{1,0:T(8,128)(2,1)} async-done(((bf16[64,3328]{1,0:T(8,128)(2,1)}), bf16[2048,3328]{1,0:T(8,128)(2,1)}) %all-gather.2.cloned.1.call-update) | async-done | bytes 13631504 | tf_op jit(solution)/shard_map/all_gather | solution.py:12
  98.4 12.3 %all-to-all-start.1 = ((bf16[128,16,64]{0,2,1:T(8,128)(2,1)}), bf16[128,16,64]{0,2,1:T(8,128)(2,1)S(1)}, u32[]{:S(2)}, u32[]{:S(2)}) async-start(bf16[128,16,64]{0,2,1:T(8,128)(2,1)} %bitcast.15), calls=%async_computation.1 | async-start | bytes 524288 | tf_op jit(solution)/shard_map/all_to_all | solution.py:86
  114.8 14.4 %all-to-all-done.1 = bf16[128,16,64]{0,2,1:T(8,128)(2,1)S(1)} async-done(((bf16[128,16,64]{0,2,1:T(8,128)(2,1)}), bf16[128,16,64]{0,2,1:T(8,128)(2,1)S(1)}, u32[]{:S(2)}, u32[]{:S(2)}) %all-to-all-start.1) | async-done | bytes 262176 | tf_op jit(solution)/shard_map/all_to_all | solution.py:86
  129.3 6.0 all-to-all-start.4
  139.5 14.1 %all-to-all-done.4 = bf16[128,16,64]{0,2,1:T(8,128)(2,1)S(1)} async-done(((bf16[128,16,64]{0,2,1:T(8,128)(2,1)}), bf16[128,16,64]{0,2,1:T(8,128)(2,1)S(1)}, u32[]{:S(2)}, u32[]{:S(2)}) %all-to-all-start.4) | async-done | bytes 262176 | tf_op jit(solution)/shard_map/all_to_all | solution.py:85
  153.6 5.9 all-to-all-start.3
  163.7 14.3 %all-to-all-done.3 = bf16[128,16,64]{0,2,1:T(8,128)(2,1)S(1)} async-done(((bf16[128,16,64]{0,2,1:T(8,128)(2,1)}), bf16[128,16,64]{0,2,1:T(8,128)(2,1)S(1)}, u32[]{:S(2)}, u32[]{:S(2)}) %all-to-all-start.3) | async-done | bytes 262176 | tf_op jit(solution)/shard_map/all_to_all | solution.py:84
  178.0 5.6 all-to-all-start
  184.9 17.2 %all-to-all-done = bf16[128,16,64]{0,2,1:T(8,128)(2,1)S(1)} async-done(((bf16[128,16,64]{0,2,1:T(8,128)(2,1)}), bf16[128,16,64]{0,2,1:T(8,128)(2,1)S(1)}, u32[]{:S(2)}, u32[]{:S(2)}) %all-to-all-start) | async-done | bytes 262176 | tf_op jit(solution)/shard_map/all_to_all | solution.py:83
  212.9 5.7 reverse.14
  227.1 6.7 reverse.13
  239.3 6.7 reverse.12
  262.0 7.6 %fusion.87 = f32[2,32,64,64]{3,2,1,0:T(8,128)} fusion(f32[1,32,64,64]{3,2,1,0:T(8,128)S(1)} %bitcast.228, f32[1,32,64,64]{3,2,1,0:T(8,128)S(1)} %bitcast.225, f32[2,1,32,64,64]{4,2,3,1,0:T(8,128)S(1)} %fusion.117, f32[2,32,64]{2,1,0:T(8,128)S(1)} %get-tuple-element.72, f32[1,32,64,64]{3,2,1,0:T(8,128)S(1)} %bitcast.241, ...), kind=kOutput, calls=%fused_computation.119 | convolution fusion | flops 203161600 | bytes 4211200 | tf_op jit(solution)/shard_map/...tn,...jn->...tj/dot_general | solution.py:20
  269.6 7.8 %fusion.89 = f32[2,32,64,64]{3,2,1,0:T(8,128)} fusion(f32[1,32,64,64]{3,2,1,0:T(8,128)S(1)} %bitcast.229, f32[1,32,64,64]{3,2,1,0:T(8,128)S(1)} %bitcast.226, f32[2,1,32,64,64]{4,2,3,1,0:T(8,128)S(1)} %fusion.117, f32[2,32,64]{2,1,0:T(8,128)S(1)} %get-tuple-element.72, f32[2,64]{1,0:T(2,128)S(1)} %add_divide_fusion, f32[1,32,64,64]{3,2,1,0:T(8,128)S(1)} %bitcast.236, ...), kind=kOutput, calls=%fused_computation.120 | convolution fusion | flops 203161600 | bytes 4211200 | tf_op jit(solution)/shard_map/...tn,...jn->...tj/dot_general | solution.py:20
  277.4 8.0 %fusion.85 = f32[2,32,64,64]{3,2,1,0:T(8,128)} fusion(f32[2,32,64]{2,1,0:T(8,128)S(1)} %get-tuple-element.72, f32[1,32,64,64]{3,2,1,0:T(8,128)S(1)} %bitcast.237, f32[1,32,64,64]{3,2,1,0:T(8,128)S(1)} %broadcast_divide_fusion, f32[1,32,64,64]{3,2,1,0:T(8,128)S(1)} %bitcast.242, f32[1,32,64,64]{3,2,1,0:T(8,128)S(1)} %bitcast.233, ...), kind=kOutput, calls=%fused_computation.117 | convolution fusion | flops 204996608 | bytes 5259776 | tf_op jit(solution)/shard_map/...tn,...jn->...tj/dot_general | solution.py:20
  285.4 8.3 %fusion.86 = f32[2,32,64,64]{3,2,1,0:T(8,128)} fusion(f32[2,32,64]{2,1,0:T(8,128)S(1)} %get-tuple-element.72, f32[1,32,64,64]{3,2,1,0:T(8,128)S(1)} %bitcast.238, f32[1,32,64,64]{3,2,1,0:T(8,128)S(1)} %broadcast_divide_fusion, f32[2,1,32,64,64]{4,2,3,1,0:T(8,128)S(1)} %fusion.117, f32[2,64]{1,0:T(2,128)S(1)} %add_divide_fusion, ...), kind=kOutput, calls=%fused_computation.118 | convolution fusion | flops 204996608 | bytes 4211200 | tf_op jit(solution)/shard_map/...tn,...jn->...tj/dot_general | solution.py:20
  315.8 7.9 %broadcast_select_fusion.1 = (f32[2,32,64,64]{1,3,2,0:T(8,128)}, f32[2,1,32,1,64,64]{2,5,4,3,1,0:T(8,128)}) fusion(f32[2,32,64,64]{1,3,2,0:T(8,128)} %copy.210, pred[64,64]{1,0:T(8,128)(4,1)S(1)} %get-tuple-element.87, f32[64,64]{1,0:T(8,128)S(1)} %fusion.96, f32[2,32,64,64]{1,3,2,0:T(8,128)} %copy.196, f32[64,64]{1,0:T(8,128)S(1)} %get-tuple-element.88), kind=kLoop, calls=%fused_computation.54 | loop fusion | flops 1310720 | bytes 4231168 | tf_op jit(solution)/shard_map/jit(_where)/select_n | solution.py:137
  331.7 6.4 broadcast_select_fusion
  346.3 134.0 %custom-call.3 = f32[2,1,32,1,64,64]{2,4,5,3,1,0:T(8,128)} custom-call(f32[2,1,32,1,64,64]{2,5,4,3,1,0:T(8,128)} %get-tuple-element.80), custom_call_target="InvertDiagBlocksLowerTriangular" | custom-call | tf_op jit(solution)/shard_map/triangular_solve | solution.py:141
  495.7 6.5 fusion.80
  534.3 84.6 %while.12 = (s32[]{:T(128)}, f32[2,1,64,64]{2,3,0,1:T(8,128)S(1)}, f32[32,2,1,64,64]{3,4,1,2,0:T(8,128)}, f32[32,2,1,64,64]{3,4,1,2,0:T(8,128)}, f32[32,2,1,64,64]{4,3,0,1,2:T(8,128)}, /*index=5*/s32[]{:T(128)}) while((s32[]{:T(128)}, f32[2,1,64,64]{2,3,0,1:T(8,128)S(1)}, f32[32,2,1,64,64]{3,4,1,2,0:T(8,128)}, ...), condition=%wide.region_3.4_spmd, body=%wide.region_2.3_spmd.sunk | while | flops 6299650 | bytes 458841 | solution.py:162
  619.0 6.8 %fusion.35 = f32[2,32,64,64]{3,2,1,0:T(8,128)S(1)} fusion(f32[1,32,64,64]{3,2,1,0:T(8,128)} %bitcast.235, f32[1,32,64,64]{3,2,1,0:T(8,128)} %copy-done.15, f32[1,32,64,64]{3,2,1,0:T(8,128)} %bitcast.254, f32[1,32,64,64]{3,2,1,0:T(8,128)} %bitcast.250, f32[2,1,32,64,64]{4,2,3,1,0:T(8,128)S(1)} %fusion.117, f32[32,2,1,64,64]{3,4,1,2,0:T(8,128)} %get-tuple-element.32), kind=kOutput, calls=%fused_computation.58 | convolution fusion | flops 203685888 | bytes 5242880 | tf_op jit(solution)/shard_map/...tk,...vk->...tv/dot_general | solution.py:20
  636.4 6.8 %rev.12 = f32[2048,1,64]{2,0,1:T(8,128)S(1)} reverse(f32[2048,1,64]{2,0,1:T(8,128)} %bitcast.247), dimensions={0} | reverse | bytes 1048576 | tf_op jit(solution)/shard_map/jit(_flip)/rev | solution.py:180
  647.8 24.7 %all_to_all.78 = bf16[16,128,64]{1,2,0:T(8,128)(2,1)S(1)} all-to-all(bf16[16,128,64]{1,2,0:T(8,128)(2,1)S(1)} %copy_bitcast_fusion.4), channel_id=1, replica_groups=mesh['sp'=16,'dp'=32] {'sp'}, dimensions={0} | all-to-all | bytes 524288 | tf_op jit(solution)/shard_map/all_to_all | solution.py:199
  (322 shorter events, 245.0 us)
Async XLA Ops:
  6.5 89.0 %copy-start = (bf16[1,128,2048]{2,1,0:T(8,128)(2,1)S(1)}, bf16[1,128,2048]{2,1,0:T(8,128)(2,1)}, u32[]{:S(2)}) copy-start(bf16[1,128,2048]{2,1,0:T(8,128)(2,1)} %param.12) | copy-start | bytes 1572868
  6.5 90.7 %copy-start.32 = (bf16[2,128,1024]{2,1,0:T(8,128)(2,1)S(1)}, bf16[2,128,1024]{2,1,0:T(8,128)(2,1)}, u32[]{:S(2)}) copy-start(bf16[2,128,1024]{2,1,0:T(8,128)(2,1)} %param.17) | copy-start | bytes 1572868
  6.5 89.0 %all-gather.2.cloned.1.call-start = ((), (), s32[]{:S(2)}) async-start(), calls=%async_computation.6 | async-start | bytes 14057472 | tf_op jit(solution)/shard_map/all_gather | solution.py:12
  98.4 30.9 %all-to-all-start.1 = ((bf16[128,16,64]{0,2,1:T(8,128)(2,1)}), bf16[128,16,64]{0,2,1:T(8,128)(2,1)S(1)}, u32[]{:S(2)}, u32[]{:S(2)}) async-start(bf16[128,16,64]{0,2,1:T(8,128)(2,1)} %bitcast.15), calls=%async_computation.1 | async-start | bytes 524288 | tf_op jit(solution)/shard_map/all_to_all | solution.py:86
  129.3 24.3 %all-to-all-start.4 = ((bf16[128,16,64]{0,2,1:T(8,128)(2,1)}), bf16[128,16,64]{0,2,1:T(8,128)(2,1)S(1)}, u32[]{:S(2)}, u32[]{:S(2)}) async-start(bf16[128,16,64]{0,2,1:T(8,128)(2,1)} %bitcast.38), calls=%async_computation.4 | async-start | bytes 524288 | tf_op jit(solution)/shard_map/all_to_all | solution.py:85
  153.6 24.5 %all-to-all-start.3 = ((bf16[128,16,64]{0,2,1:T(8,128)(2,1)}), bf16[128,16,64]{0,2,1:T(8,128)(2,1)S(1)}, u32[]{:S(2)}, u32[]{:S(2)}) async-start(bf16[128,16,64]{0,2,1:T(8,128)(2,1)} %bitcast.23), calls=%async_computation.3 | async-start | bytes 524288 | tf_op jit(solution)/shard_map/all_to_all | solution.py:84
  159.5 24.1 %copy-start.34 = (f32[2,64]{1,0:T(2,128)S(1)}, f32[2,64]{1,0:T(2,128)}, u32[]{:S(2)}) copy-start(f32[2,64]{1,0:T(2,128)} %param.19) | copy-start | bytes 1540
  178.0 24.1 %all-to-all-start = ((bf16[128,16,64]{0,2,1:T(8,128)(2,1)}), bf16[128,16,64]{0,2,1:T(8,128)(2,1)S(1)}, u32[]{:S(2)}, u32[]{:S(2)}) async-start(bf16[128,16,64]{0,2,1:T(8,128)(2,1)} %bitcast.8), calls=%async_computation | async-start | bytes 524288 | tf_op jit(solution)/shard_map/all_to_all | solution.py:83
  202.1 24.1 %all-to-all-start.2 = ((bf16[128,16,64]{0,2,1:T(8,128)(2,1)}), bf16[128,16,64]{0,2,1:T(8,128)(2,1)S(1)}, u32[]{:S(2)}, u32[]{:S(2)}) async-start(bf16[128,16,64]{0,2,1:T(8,128)(2,1)} %bitcast.19), calls=%async_computation.2 | async-start | bytes 524288 | tf_op jit(solution)/shard_map/all_to_all | solution.py:87
  260.4 25.0 %copy-start.15 = (f32[1,32,64,64]{3,2,1,0:T(8,128)}, f32[1,32,64,64]{3,2,1,0:T(8,128)S(1)}, u32[]{:S(2)}) copy-start(f32[1,32,64,64]{3,2,1,0:T(8,128)S(1)} %broadcast_divide_fusion) | copy-start | bytes 1572868
  262.0 7.6 %copy-start.13 = (f32[2048,1,64]{2,0,1:T(8,128)S(1)}, f32[2048,1,64]{2,0,1:T(8,128)}, u32[]{:S(2)}) copy-start(f32[2048,1,64]{2,0,1:T(8,128)} %copy.236) | copy-start | bytes 1572868
  269.6 7.8 %copy-start.28 = (f32[16,128,64]{2,1,0:T(8,128)S(1)}, f32[16,128,64]{2,1,0:T(8,128)}, u32[]{:S(2)}) copy-start(f32[16,128,64]{2,1,0:T(8,128)} %copy.237) | copy-start | bytes 1572868
  269.6 7.8 %copy-start.30 = (f32[2048,64]{1,0:T(8,128)S(1)}, f32[2048,64]{1,0:T(8,128)}, u32[]{:S(2)}) copy-start(f32[2048,64]{1,0:T(8,128)} %copy.238) | copy-start | bytes 1572868
  285.4 8.3 %copy-start.25 = (f32[16,128,64]{1,2,0:T(8,128)S(1)}, f32[16,128,64]{1,2,0:T(8,128)}, u32[]{:S(2)}) copy-start(f32[16,128,64]{1,2,0:T(8,128)} %get-tuple-element.73) | copy-start | bytes 1572868
  294.8 5.1 copy-start.24
  485.7 5.0 copy-start.14
  485.7 5.0 copy-start.16
  490.8 4.9 copy-start.29
  490.8 4.9 copy-start.31
  495.7 6.5 copy-start.2
  506.3 4.8 copy-start.20
  618.9 6.8 %copy-start.4 = (f32[2,32,64,64]{3,2,1,0:T(8,128)S(1)}, f32[2,32,64,64]{3,2,1,0:T(8,128)}, u32[]{:S(2)}) copy-start(f32[2,32,64,64]{3,2,1,0:T(8,128)} %copy-done.3) | copy-start | bytes 3145732
  618.9 6.8 %copy-start.22 = (f32[2,32,64,64]{3,2,1,0:T(8,128)S(1)}, f32[2,32,64,64]{3,2,1,0:T(8,128)}, u32[]{:S(2)}) copy-start(f32[2,32,64,64]{3,2,1,0:T(8,128)} %fusion.51) | copy-start | bytes 3145732
  645.4 27.9 %copy-start.1 = (bf16[1,128,2048]{2,1,0:T(8,128)(2,1)S(1)}, bf16[1,128,2048]{2,1,0:T(8,128)(2,1)}, u32[]{:S(2)}) copy-start(bf16[1,128,2048]{2,1,0:T(8,128)(2,1)} %param.12) | copy-start | bytes 1572868
  (18 other events, 49.2 us)
Sparse Core Ops, SparseCore 0:
  10.5 85.0 all-gather.1
where the time goes:
time: 694 us; the launch traced here: 680 us
  other arithmetic  165 us (24%)
  local copies, waits for them, and re-layouts  159 us (23%)
  waiting for transfers between devices  152 us (22%)
  matrix products  129 us (19%)
  starting transfers between devices  35.3 us (5%)
  blocking collectives  24.7 us (4%)
  between operations  14.3 us (2%)
    another operation x4, other arithmetic, per_device(): lax.linalg.triangular_solve(identity - erase_write, jnp.broadcast_to(iden...  134 us
    dot_general x46, matrix products, contract(): return jnp.einsum(pattern, former, latter, precision=lax.Precision.HIGHEST)  110 us
    all_gather x1, waiting for transfers between devices, in_one_piece(): result, at, outs = (lax.all_gather(both, axis, axis=dim, tiled=True), 0, [])  86.2 us
    dynamic_slice x64, local copies, waits for them, and re-layouts, per_device(): lax.scan(advance, start_state, (jnp.moveaxis(transfer, 2, 0), jnp.moveaxi...  29.9 us
    another operation x5, local copies, waits for them, and re-layouts  25.8 us
    all_to_all x1, blocking collectives, per_device(): lax.all_to_all(mixed, 'sp', split_axis=0, concat_axis=1, tiled=True)  24.7 us
    dynamic_update_slice x32, local copies, waits for them, and re-layouts, per_device(): lax.scan(advance, start_state, (jnp.moveaxis(transfer, 2, 0), jnp.moveaxi...  20.4 us
    dot_general x5, local copies, waits for them, and re-layouts, contract(): return jnp.einsum(pattern, former, latter, precision=lax.Precision.HIGHEST)  19.3 us
  transfers between devices with their start and end apart: 6, of which 6 were waited for; matrix products, arithmetic and copies ran while one was open for 4% of the time, Pallas kernels for 0%

commit v1 on v0

--- a/solution.py
+++ b/solution.py
@@ -5,6 +5,13 @@
 from jax.sharding import PartitionSpec as P
 
 SUBSPACE_SIZE = 64
+
+
+def exchange_blocks(block, axis, split, join):
+    size = lax.axis_size(axis)
+    parts = jnp.stack(jnp.split(block, size, axis=split), axis=0)
+    parts = lax.all_to_all(parts, axis, split_axis=0, concat_axis=0)
+    return jnp.concatenate(parts, axis=join)
 
 
 def in_one_piece(arrays, axis, dim, along):
@@ -82,7 +89,7 @@
     moved = (
         lax.all_to_all(receive, "sp", split_axis=1, concat_axis=0, tiled=True),
         lax.all_to_all(key_rows, "sp", split_axis=1, concat_axis=0, tiled=True),
-        lax.all_to_all(value_rows, "sp", split_axis=1, concat_axis=0, tiled=True),
+        exchange_blocks(value_rows, "sp", 1, 0),
         lax.all_to_all(forward_pre, "sp", split_axis=1, concat_axis=0, tiled=True),
         lax.all_to_all(backward_pre, "sp", split_axis=1, concat_axis=0, tiled=True),
     )

time: 694 us -> 695 us (level)
  waiting for transfers between devices: 152 us -> 142 us
  local copies, waits for them, and re-layouts: 159 us -> 168 us
    unnamed x72 -> x93, local copies, waits for them, and re-layouts: 3.51 us -> 12.5 us
    all_to_all x1, waiting for transfers between devices: 14.4 us -> 5.52 us  [per_device(): lax.all_to_all(forward_pre, 'sp', split_axis=1, concat_axis=0, tiled=True)]
    another operation x5 -> x6, local copies, waits for them, and re-layouts: 25.8 us -> 26.4 us
    convert_element_type x13 -> x12, local copies, waits for them, and re-layouts: 14 us -> 13.7 us  [by_head(): content_matrix_full.astype(jnp.float32)]
  transfers between devices with their start and end apart: 6 -> 6, of which waited for: 6 -> 6; matrix products, arithmetic and copies ran while one was open for 4% -> 5% of each run, Pallas kernels for 0% -> 0%
where the time goes in v1:
time: 695 us; the launch traced here: 681 us
  local copies, waits for them, and re-layouts  168 us (24%)
  other arithmetic  167 us (24%)
  waiting for transfers between devices  142 us (20%)
  matrix products  128 us (18%)
  starting transfers between devices  35.5 us (5%)
  blocking collectives  23.9 us (3%)
  between operations  14.3 us (2%)
    another operation x4, other arithmetic, per_device(): lax.linalg.triangular_solve(identity - erase_write, jnp.broadcast_to(iden...  135 us
    dot_general x46, matrix products, contract(): return jnp.einsum(pattern, former, latter, precision=lax.Precision.HIGHEST)  111 us
    all_gather x1, waiting for transfers between devices, in_one_piece(): result, at, outs = (lax.all_gather(both, axis, axis=dim, tiled=True), 0, [])  86.2 us
    dynamic_slice x64, local copies, waits for them, and re-layouts, per_device(): lax.scan(advance, start_state, (jnp.moveaxis(transfer, 2, 0), jnp.moveaxi...  29.9 us
    another operation x5, local copies, waits for them, and re-layouts  25.8 us
    all_to_all x1, blocking collectives, per_device(): lax.all_to_all(mixed, 'sp', split_axis=0, concat_axis=1, tiled=True)  23.9 us
    dynamic_update_slice x32, local copies, waits for them, and re-layouts, per_device(): lax.scan(advance, start_state, (jnp.moveaxis(transfer, 2, 0), jnp.moveaxi...  20.3 us
    dot_general x5, local copies, waits for them, and re-layouts, contract(): return jnp.einsum(pattern, former, latter, precision=lax.Precision.HIGHEST)  19.3 us
  transfers between devices with their start and end apart: 6, of which 6 were waited for; matrix products, arithmetic and copies ran while one was open for 5% of the time, Pallas kernels for 0%

profile of v1, /device:TPU:2, one launch (start us, length us, event | category | flops | bytes accessed | tf_op | source)
XLA Modules:
  0.0 680.8 jit_solution(223557860400539103)
XLA Ops:
  9.3 86.2 %all-gather.2.cloned.1.call-done = bf16[2048,3328]{1,0:T(8,128)(2,1)} async-done(((bf16[64,3328]{1,0:T(8,128)(2,1)}), bf16[2048,3328]{1,0:T(8,128)(2,1)}) %all-gather.2.cloned.1.call-update) | async-done | bytes 13631504 | tf_op jit(solution)/shard_map/all_gather | solution.py:19
  98.4 12.3 %all-to-all-start.1 = ((bf16[128,16,64]{0,2,1:T(8,128)(2,1)}), bf16[128,16,64]{0,2,1:T(8,128)(2,1)S(1)}, u32[]{:S(2)}, u32[]{:S(2)}) async-start(bf16[128,16,64]{0,2,1:T(8,128)(2,1)} %bitcast.15), calls=%async_computation.1 | async-start | bytes 524288 | tf_op jit(solution)/shard_map/all_to_all | solution.py:93
  129.3 6.5 all-to-all-start.4
  140.0 14.2 %all-to-all-done.4 = bf16[16,128,64]{1,2,0:T(8,128)(2,1)S(1)} async-done(((bf16[16,128,64]{1,2,0:T(8,128)(2,1)}), bf16[16,128,64]{1,2,0:T(8,128)(2,1)S(1)}, u32[]{:S(2)}, u32[]{:S(2)}) %all-to-all-start.4) | async-done | bytes 262176 | tf_op jit(solution)/shard_map/all_to_all | solution.py:13
  154.2 5.6 all-to-all-start.3
  165.2 13.1 %all-to-all-done.3 = bf16[128,16,64]{0,2,1:T(8,128)(2,1)S(1)} async-done(((bf16[128,16,64]{0,2,1:T(8,128)(2,1)}), bf16[128,16,64]{0,2,1:T(8,128)(2,1)S(1)}, u32[]{:S(2)}, u32[]{:S(2)}) %all-to-all-start.3) | async-done | bytes 262176 | tf_op jit(solution)/shard_map/all_to_all | solution.py:91
  185.7 16.7 %all-to-all-done = bf16[128,16,64]{0,2,1:T(8,128)(2,1)S(1)} async-done(((bf16[128,16,64]{0,2,1:T(8,128)(2,1)}), bf16[128,16,64]{0,2,1:T(8,128)(2,1)S(1)}, u32[]{:S(2)}, u32[]{:S(2)}) %all-to-all-start) | async-done | bytes 262176 | tf_op jit(solution)/shard_map/all_to_all | solution.py:90
  202.4 5.6 all-to-all-start.2
  208.1 5.6 reverse.14
  220.2 6.4 all-to-all-done.2
  228.4 6.7 reverse.13
  240.6 6.7 reverse.12
  263.3 7.6 %fusion.90 = f32[2,32,64,64]{3,2,1,0:T(8,128)} fusion(f32[1,32,64,64]{3,2,1,0:T(8,128)S(1)} %bitcast.289, f32[1,32,64,64]{3,2,1,0:T(8,128)S(1)} %bitcast.286, f32[2,1,32,64,64]{4,2,3,1,0:T(8,128)S(1)} %fusion.120, f32[2,32,64]{2,1,0:T(8,128)S(1)} %get-tuple-element.72, f32[1,32,64,64]{3,2,1,0:T(8,128)S(1)} %bitcast.302, ...), kind=kOutput, calls=%fused_computation.118 | convolution fusion | flops 203161600 | bytes 4211200 | tf_op jit(solution)/shard_map/...tn,...jn->...tj/dot_general | solution.py:27
  271.0 7.8 %fusion.92 = f32[2,32,64,64]{3,2,1,0:T(8,128)} fusion(f32[1,32,64,64]{3,2,1,0:T(8,128)S(1)} %bitcast.290, f32[1,32,64,64]{3,2,1,0:T(8,128)S(1)} %bitcast.287, f32[2,1,32,64,64]{4,2,3,1,0:T(8,128)S(1)} %fusion.120, f32[2,32,64]{2,1,0:T(8,128)S(1)} %get-tuple-element.72, f32[2,64]{1,0:T(2,128)S(1)} %copy-done.32, f32[1,32,64,64]{3,2,1,0:T(8,128)S(1)} %bitcast.297, ...), kind=kOutput, calls=%fused_computation.119 | convolution fusion | flops 203161600 | bytes 4211200 | tf_op jit(solution)/shard_map/...tn,...jn->...tj/dot_general | solution.py:27
  278.8 8.0 %fusion.88 = f32[2,32,64,64]{3,2,1,0:T(8,128)} fusion(f32[2,32,64]{2,1,0:T(8,128)S(1)} %get-tuple-element.72, f32[1,32,64,64]{3,2,1,0:T(8,128)S(1)} %bitcast.298, f32[1,32,64,64]{3,2,1,0:T(8,128)S(1)} %broadcast_divide_fusion, f32[1,32,64,64]{3,2,1,0:T(8,128)S(1)} %bitcast.303, f32[1,32,64,64]{3,2,1,0:T(8,128)S(1)} %bitcast.294, ...), kind=kOutput, calls=%fused_computation.116 | convolution fusion | flops 204996608 | bytes 5259776 | tf_op jit(solution)/shard_map/...tn,...jn->...tj/dot_general | solution.py:27
  286.8 8.3 %fusion.89 = f32[2,32,64,64]{3,2,1,0:T(8,128)} fusion(f32[2,32,64]{2,1,0:T(8,128)S(1)} %get-tuple-element.72, f32[1,32,64,64]{3,2,1,0:T(8,128)S(1)} %bitcast.299, f32[1,32,64,64]{3,2,1,0:T(8,128)S(1)} %broadcast_divide_fusion, f32[2,1,32,64,64]{4,2,3,1,0:T(8,128)S(1)} %fusion.120, f32[2,64]{1,0:T(2,128)S(1)} %copy-done.32, ...), kind=kOutput, calls=%fused_computation.117 | convolution fusion | flops 204996608 | bytes 4211200 | tf_op jit(solution)/shard_map/...tn,...jn->...tj/dot_general | solution.py:27
  317.0 7.8 %broadcast_select_fusion.1 = (f32[2,32,64,64]{1,3,2,0:T(8,128)}, f32[2,1,32,1,64,64]{2,5,4,3,1,0:T(8,128)}) fusion(f32[2,32,64,64]{1,3,2,0:T(8,128)} %copy.211, pred[64,64]{1,0:T(8,128)(4,1)S(1)} %copy-done.35, f32[64,64]{1,0:T(8,128)S(1)} %fusion.99, f32[2,32,64,64]{1,3,2,0:T(8,128)} %copy.197, f32[64,64]{1,0:T(8,128)S(1)} %get-tuple-element.86), kind=kLoop, calls=%fused_computation.54 | loop fusion | flops 1310720 | bytes 4231168 | tf_op jit(solution)/shard_map/jit(_where)/select_n | solution.py:144
  332.8 6.4 broadcast_select_fusion
  347.4 134.0 %custom-call.3 = f32[2,1,32,1,64,64]{2,4,5,3,1,0:T(8,128)} custom-call(f32[2,1,32,1,64,64]{2,5,4,3,1,0:T(8,128)} %get-tuple-element.78), custom_call_target="InvertDiagBlocksLowerTriangular" | custom-call | tf_op jit(solution)/shard_map/triangular_solve | solution.py:148
  496.9 6.5 fusion.83
  535.5 84.6 %while.12 = (s32[]{:T(128)}, f32[2,1,64,64]{2,3,0,1:T(8,128)S(1)}, f32[32,2,1,64,64]{3,4,1,2,0:T(8,128)}, f32[32,2,1,64,64]{3,4,1,2,0:T(8,128)}, f32[32,2,1,64,64]{4,3,0,1,2:T(8,128)}, /*index=5*/s32[]{:T(128)}) while((s32[]{:T(128)}, f32[2,1,64,64]{2,3,0,1:T(8,128)S(1)}, f32[32,2,1,64,64]{3,4,1,2,0:T(8,128)}, ...), condition=%wide.region_3.4_spmd, body=%wide.region_2.3_spmd.sunk | while | flops 6299650 | bytes 458841 | solution.py:169
  620.2 6.8 %fusion.35 = f32[2,32,64,64]{3,2,1,0:T(8,128)S(1)} fusion(f32[1,32,64,64]{3,2,1,0:T(8,128)} %bitcast.296, f32[1,32,64,64]{3,2,1,0:T(8,128)} %copy-done.15, f32[1,32,64,64]{3,2,1,0:T(8,128)} %bitcast.313, f32[1,32,64,64]{3,2,1,0:T(8,128)} %bitcast.309, f32[2,1,32,64,64]{4,2,3,1,0:T(8,128)S(1)} %fusion.120, f32[32,2,1,64,64]{3,4,1,2,0:T(8,128)} %get-tuple-element.32), kind=kOutput, calls=%fused_computation.58 | convolution fusion | flops 203685888 | bytes 5242880 | tf_op jit(solution)/shard_map/...tk,...vk->...tv/dot_general | solution.py:27
  637.6 6.8 %rev.12 = f32[2048,1,64]{2,0,1:T(8,128)S(1)} reverse(f32[2048,1,64]{2,0,1:T(8,128)} %bitcast.306), dimensions={0} | reverse | bytes 1048576 | tf_op jit(solution)/shard_map/jit(_flip)/rev | solution.py:187
  649.0 23.9 %all_to_all.70 = bf16[16,128,64]{1,2,0:T(8,128)(2,1)S(1)} all-to-all(bf16[16,128,64]{1,2,0:T(8,128)(2,1)S(1)} %copy_bitcast_fusion.4), channel_id=1, replica_groups=mesh['sp'=16,'dp'=32] {'sp'}, dimensions={0} | all-to-all | bytes 524288 | tf_op jit(solution)/shard_map/all_to_all | solution.py:206
  (343 shorter events, 255.5 us)
Async XLA Ops:
  6.5 89.0 %copy-start = (bf16[1,128,2048]{2,1,0:T(8,128)(2,1)S(1)}, bf16[1,128,2048]{2,1,0:T(8,128)(2,1)}, u32[]{:S(2)}) copy-start(bf16[1,128,2048]{2,1,0:T(8,128)(2,1)} %param.12) | copy-start | bytes 1572868
  6.5 90.7 %copy-start.31 = (bf16[2,128,1024]{2,1,0:T(8,128)(2,1)S(1)}, bf16[2,128,1024]{2,1,0:T(8,128)(2,1)}, u32[]{:S(2)}) copy-start(bf16[2,128,1024]{2,1,0:T(8,128)(2,1)} %param.17) | copy-start | bytes 1572868
  6.5 89.0 %all-gather.2.cloned.1.call-start = ((), (), s32[]{:S(2)}) async-start(), calls=%async_computation.6 | async-start | bytes 14057472 | tf_op jit(solution)/shard_map/all_gather | solution.py:19
  98.4 30.9 %all-to-all-start.1 = ((bf16[128,16,64]{0,2,1:T(8,128)(2,1)}), bf16[128,16,64]{0,2,1:T(8,128)(2,1)S(1)}, u32[]{:S(2)}, u32[]{:S(2)}) async-start(bf16[128,16,64]{0,2,1:T(8,128)(2,1)} %bitcast.15), calls=%async_computation.1 | async-start | bytes 524288 | tf_op jit(solution)/shard_map/all_to_all | solution.py:93
  129.3 25.0 %all-to-all-start.4 = ((bf16[16,128,64]{1,2,0:T(8,128)(2,1)}), bf16[16,128,64]{1,2,0:T(8,128)(2,1)S(1)}, u32[]{:S(2)}, u32[]{:S(2)}) async-start(bf16[16,128,64]{1,2,0:T(8,128)(2,1)} %constant_dynamic-update-slice_fusion), calls=%async_computation.4 | async-start | bytes 524288 | tf_op jit(solution)/shard_map/all_to_all | solution.py:13
  135.8 24.6 %copy-start.37 = (f32[2,64]{1,0:T(2,128)S(1)}, f32[2,64]{1,0:T(2,128)}, u32[]{:S(2)}) copy-start(f32[2,64]{1,0:T(2,128)} %param.19) | copy-start | bytes 1540
  154.2 24.1 %all-to-all-start.3 = ((bf16[128,16,64]{0,2,1:T(8,128)(2,1)}), bf16[128,16,64]{0,2,1:T(8,128)(2,1)S(1)}, u32[]{:S(2)}, u32[]{:S(2)}) async-start(bf16[128,16,64]{0,2,1:T(8,128)(2,1)} %bitcast.23), calls=%async_computation.3 | async-start | bytes 524288 | tf_op jit(solution)/shard_map/all_to_all | solution.py:91
  178.3 24.1 %all-to-all-start = ((bf16[128,16,64]{0,2,1:T(8,128)(2,1)}), bf16[128,16,64]{0,2,1:T(8,128)(2,1)S(1)}, u32[]{:S(2)}, u32[]{:S(2)}) async-start(bf16[128,16,64]{0,2,1:T(8,128)(2,1)} %bitcast.8), calls=%async_computation | async-start | bytes 524288 | tf_op jit(solution)/shard_map/all_to_all | solution.py:90
  202.4 24.2 %all-to-all-start.2 = ((bf16[128,16,64]{0,2,1:T(8,128)(2,1)}), bf16[128,16,64]{0,2,1:T(8,128)(2,1)}, u32[]{:S(2)}, u32[]{:S(2)}) async-start(bf16[128,16,64]{0,2,1:T(8,128)(2,1)} %bitcast.19), calls=%async_computation.2 | async-start | bytes 524288 | tf_op jit(solution)/shard_map/all_to_all | solution.py:94
  239.3 9.4 %copy-start.25 = (f32[16,8,8,128]{3,2,0,1:T(8,128)S(1)}, f32[16,8,8,128]{3,2,0,1:T(8,128)}, u32[]{:S(2)}) copy-start(f32[16,8,8,128]{3,2,0,1:T(8,128)} %copy.303) | copy-start | bytes 1572868
  261.8 25.0 %copy-start.15 = (f32[1,32,64,64]{3,2,1,0:T(8,128)}, f32[1,32,64,64]{3,2,1,0:T(8,128)S(1)}, u32[]{:S(2)}) copy-start(f32[1,32,64,64]{3,2,1,0:T(8,128)S(1)} %broadcast_divide_fusion) | copy-start | bytes 1572868
  263.3 7.6 %copy-start.13 = (f32[2048,1,64]{2,0,1:T(8,128)S(1)}, f32[2048,1,64]{2,0,1:T(8,128)}, u32[]{:S(2)}) copy-start(f32[2048,1,64]{2,0,1:T(8,128)} %copy.237) | copy-start | bytes 1572868
  271.0 7.8 %copy-start.27 = (f32[16,128,64]{2,1,0:T(8,128)S(1)}, f32[16,128,64]{2,1,0:T(8,128)}, u32[]{:S(2)}) copy-start(f32[16,128,64]{2,1,0:T(8,128)} %copy.238) | copy-start | bytes 1572868
  271.0 7.8 %copy-start.29 = (f32[2048,64]{1,0:T(8,128)S(1)}, f32[2048,64]{1,0:T(8,128)}, u32[]{:S(2)}) copy-start(f32[2048,64]{1,0:T(8,128)} %copy.239) | copy-start | bytes 1572868
  295.1 6.0 copy-start.24
  486.9 5.0 copy-start.14
  486.9 5.0 copy-start.16
  486.9 5.0 copy-start.33
  491.9 4.9 copy-start.28
  491.9 4.9 copy-start.30
  496.9 6.5 copy-start.2
  620.1 6.8 %copy-start.4 = (f32[2,32,64,64]{3,2,1,0:T(8,128)S(1)}, f32[2,32,64,64]{3,2,1,0:T(8,128)}, u32[]{:S(2)}) copy-start(f32[2,32,64,64]{3,2,1,0:T(8,128)} %copy-done.3) | copy-start | bytes 3145732
  620.1 6.8 %copy-start.22 = (f32[2,32,64,64]{3,2,1,0:T(8,128)S(1)}, f32[2,32,64,64]{3,2,1,0:T(8,128)}, u32[]{:S(2)}) copy-start(f32[2,32,64,64]{3,2,1,0:T(8,128)} %fusion.51) | copy-start | bytes 3145732
  646.6 27.1 %copy-start.1 = (bf16[1,128,2048]{2,1,0:T(8,128)(2,1)S(1)}, bf16[1,128,2048]{2,1,0:T(8,128)(2,1)}, u32[]{:S(2)}) copy-start(bf16[1,128,2048]{2,1,0:T(8,128)(2,1)} %param.12) | copy-start | bytes 1572868
  (21 other events, 59.9 us)
Sparse Core Ops, SparseCore 0:
  10.5 85.0 all-gather.1
